TPU v7x, 32 devices: a whole 2x2x4 slice. The times are simulated.
32 devices in a mesh: sp: 8 (over z, x), tp: 4 (over y, core).
Axes of the slice: x: 2, y: 2, z: 4, core: 2. Of those that a mesh axis runs over, the one named last changes fastest.
Arguments:
- result_cotangent_values: bfloat16 [1024, 2048], P('sp'), may hold values from -6 to 6
- specialist_entry_vectors: bfloat16 [1024, 2048], P('sp'), may hold values from -6 to 6
- chosen_specialists: int32 [1024, 2], P('sp'), may hold values from 0 to 3, all different within a row; in each aligned block of 128 rows (0 to 127, 128 to 255, ...) at most 128 rows name the same one
- specialist_mixing_shares: float32 [1024, 2], P('sp'), may hold values from 0.1 to 0.9
- specialist_switch_maps: bfloat16 [8, 2048, 1792], P('sp', None, 'tp'), may hold values from -0.125 to 0.125
- specialist_widen_maps: bfloat16 [8, 2048, 1792], P('sp', None, 'tp'), may hold values from -0.125 to 0.125
- specialist_shrink_maps: bfloat16 [8, 1792, 2048], P('sp', 'tp'), may hold values from -0.09375 to 0.09375
- memory_readout_map: bfloat16 [2048, 2048], P('sp', 'tp'), may hold values from -0.125 to 0.125
- memory_source_vectors: bfloat16 [1024, 2048], P('sp', 'tp'), may hold values from -6 to 6
- memory_hidden_values: bfloat16 [1024, 2048], P('sp', 'tp'), may hold values from -6 to 6
- feature_fading_speed: float32 [2048], P('tp'), may hold values from 1.6276042e-05 to 0.009
- extra_log_fading: float32 [1024], P('sp'), may hold values from -2.8 to 0
- memory_switch_tiles: bfloat16 [8, 256, 256], P('tp'), may hold values from -0.375 to 0.375
- entry_switch_tiles: bfloat16 [8, 256, 256], P('tp'), may hold values from -0.375 to 0.375
Outputs:
- gate_proj_grad: bfloat16 [8, 2048, 1792], P('sp', None, 'tp')
- up_proj_grad: bfloat16 [8, 2048, 1792], P('sp', None, 'tp')
- down_proj_grad: bfloat16 [8, 1792, 2048], P('sp', 'tp')
- out_proj_grad: float32 [2048, 2048], P('sp', 'tp')
- lru_input_grad: float32 [1024, 2048], P('sp', 'tp')
Inputs may be any that keep to these rules, and one draw needn't show every extreme that they name: `chosen_specialists`: each token names two different experts; among the 128 tokens of one device no expert is named more than 128 times, a bound that some block reaches on some device.
All inputs are finite; a program needn't handle non-finite values.
Results may differ from a plain program's by a relative error of at most 0.009.
Values may be sent and summed in bfloat16 or wider, within the bound.
A program may use at most 128 MiB of HBM per device.

v0:
```python
import jax
import jax.numpy as jnp
from jax import lax
from jax.sharding import PartitionSpec as P

SLICES = 2


def prefix(part, axis, combine, identity):
    count = lax.axis_size(axis)
    place = lax.axis_index(axis)
    ahead = count - 1 - place
    gathered = jax.tree.map(lambda a: lax.all_gather(a, axis), part)
    state = jax.tree.map(lambda a, e: jnp.zeros_like(a) + jnp.asarray(e, a.dtype), part, identity)

    def one(turn, state):
        source = count - 1 - turn
        return combine(
            state, jax.tree.map(lambda a: lax.dynamic_index_in_dim(a, source, 0, False), gathered)
        )

    return lax.fori_loop(0, ahead, one, state)


def silu_slope(value):
    sig_value = jax.nn.sigmoid(value)
    return sig_value * (1.0 + value * (1.0 - sig_value))


def compose(upper_map, lower_map):
    return (lower_map[0] * upper_map[0], lower_map[1] + lower_map[0] * upper_map[1])


def chain_join(higher_map, lower_map):
    return (lower_map[0] * higher_map[0], lower_map[1] + lower_map[0] * higher_map[1])


def expert_backward(inputs, grads_in, gate_weight, up_weight, down_weight):
    gate_value = jnp.dot(inputs, gate_weight, preferred_element_type=jnp.float32)
    up_value = jnp.dot(inputs, up_weight, preferred_element_type=jnp.float32)
    active = jax.nn.silu(gate_value)
    hidden = (active * up_value).astype(jnp.bfloat16)
    down_grad = jnp.einsum(
        "rf,rd->fd", hidden, grads_in, preferred_element_type=jnp.float32
    ).astype(jnp.bfloat16)
    hidden_grad = jnp.einsum("rd,fd->rf", grads_in, down_weight, preferred_element_type=jnp.float32)
    gate_grad = (hidden_grad * up_value * silu_slope(gate_value)).astype(jnp.bfloat16)
    up_grad = (hidden_grad * active).astype(jnp.bfloat16)
    gate_weight_grad = jnp.einsum(
        "rd,rf->df", inputs, gate_grad, preferred_element_type=jnp.float32
    ).astype(jnp.bfloat16)
    up_weight_grad = jnp.einsum(
        "rd,rf->df", inputs, up_grad, preferred_element_type=jnp.float32
    ).astype(jnp.bfloat16)
    token_part = jnp.einsum("rf,df->rd", gate_grad, gate_weight, preferred_element_type=jnp.float32)
    token_part = token_part + jnp.einsum(
        "rf,df->rd", up_grad, up_weight, preferred_element_type=jnp.float32
    )
    return (gate_weight_grad, up_weight_grad, down_grad, token_part)


def collect(returned, targets, route_count):
    gathered = jnp.take(returned, targets[0], axis=0).astype(jnp.float32)
    for target in targets[1:]:
        gathered = gathered + jnp.take(returned, target, axis=0).astype(jnp.float32)
    return gathered.reshape(-1, route_count, gathered.shape[-1]).sum(axis=1)


def fill_slots(values, targets, slot_rows):
    buffer = jnp.zeros((slot_rows, values.shape[1]), jnp.bfloat16)
    for target in targets:
        buffer = buffer.at[target].set(values)
    return buffer


def local(
    result_cotangent_values,
    specialist_entry_vectors,
    chosen_specialists,
    specialist_mixing_shares,
    specialist_switch_maps,
    specialist_widen_maps,
    specialist_shrink_maps,
    memory_readout_map,
    memory_source_vectors,
    memory_hidden_values,
    feature_fading_speed,
    extra_log_fading,
    memory_switch_tiles,
    entry_switch_tiles,
):
    tok_rows, feature_count = result_cotangent_values.shape
    route_count = chosen_specialists.shape[1]
    sp_count = lax.axis_size("sp")
    expert_count = sp_count // SLICES
    capacity = min(tok_rows, 4 * tok_rows // expert_count)
    slot_rows = sp_count * capacity
    flat_expert = chosen_specialists.reshape(-1)
    onehot = (flat_expert[:, None] == jnp.arange(expert_count, dtype=jnp.int32)[None, :]).astype(
        jnp.int32
    )
    slot_rank = jnp.sum((jnp.cumsum(onehot, axis=0) - 1) * onehot, axis=1)
    scaled = (
        (
            specialist_mixing_shares[:, :, None]
            * result_cotangent_values[:, None, :].astype(jnp.float32)
        )
        .astype(jnp.bfloat16)
        .reshape(-1, feature_count)
    )
    copies = jnp.broadcast_to(
        specialist_entry_vectors[:, None, :], (tok_rows, route_count, feature_count)
    ).reshape(-1, feature_count)
    targets = [
        (flat_expert * SLICES + slice_index) * capacity + slot_rank for slice_index in range(SLICES)
    ]
    share = feature_count // lax.axis_size("tp")
    first_col = lax.axis_index("tp") * share
    part_grad = lax.dynamic_slice_in_dim(scaled, first_col, share, 1)
    part_rows = lax.dynamic_slice_in_dim(copies, first_col, share, 1)
    send_grad = fill_slots(part_grad, targets, slot_rows)
    send_rows = fill_slots(part_rows, targets, slot_rows)
    got_grad, got_rows = (
        lax.all_to_all(
            send_grad.reshape(sp_count, capacity, share),
            "sp",
            split_axis=0,
            concat_axis=0,
            tiled=True,
        ),
        lax.all_to_all(
            send_rows.reshape(sp_count, capacity, share),
            "sp",
            split_axis=0,
            concat_axis=0,
            tiled=True,
        ),
    )
    recv_grad, recv_rows = (
        lax.all_gather(got_grad, "tp", axis=2, tiled=True),
        lax.all_gather(got_rows, "tp", axis=2, tiled=True),
    )
    inputs = recv_rows.reshape(slot_rows, feature_count)
    grads_in = recv_grad.reshape(slot_rows, feature_count)
    gate_weight_grad, up_weight_grad, down_grad, token_part = expert_backward(
        inputs,
        grads_in,
        specialist_switch_maps[0],
        specialist_widen_maps[0],
        specialist_shrink_maps[0],
    )
    returned = lax.all_to_all(
        token_part.astype(jnp.bfloat16).reshape(sp_count, capacity, feature_count),
        "sp",
        split_axis=0,
        concat_axis=0,
        tiled=True,
    )
    own_sum = collect(returned.reshape(slot_rows, feature_count), targets, route_count)
    moe_grad = lax.psum(own_sum.astype(jnp.bfloat16), "tp").astype(jnp.float32)
    mixed_grad = (result_cotangent_values.astype(jnp.float32) + moe_grad).astype(jnp.bfloat16)
    col_count = memory_readout_map.shape[1]
    columns = mixed_grad
    upstream = jnp.dot(
        columns,
        lax.all_gather(memory_readout_map, "sp", axis=0, tiled=True),
        preferred_element_type=jnp.float32,
    )
    blocks_here = memory_switch_tiles.shape[0]
    block_width = memory_switch_tiles.shape[1]
    blocks_in = memory_source_vectors.reshape(tok_rows, blocks_here, block_width)
    memory_switch_fraction = jax.nn.sigmoid(
        jnp.einsum(
            "tnc,ncd->tnd", blocks_in, memory_switch_tiles, preferred_element_type=jnp.float32
        ).reshape(tok_rows, col_count)
    )
    inp_open = jax.nn.sigmoid(
        jnp.einsum(
            "tnc,ncd->tnd", blocks_in, entry_switch_tiles, preferred_element_type=jnp.float32
        ).reshape(tok_rows, col_count)
    )
    xin = memory_source_vectors.astype(jnp.float32)
    log_fading_factor = (
        -8.0 * memory_switch_fraction * feature_fading_speed[None, :] + extra_log_fading[:, None]
    )
    decay_mult = jnp.exp(log_fading_factor)
    spare_room = -jnp.expm1(2.0 * log_fading_factor)
    in_scale = jnp.sqrt(jnp.maximum(spare_room, 0.01))
    drive = in_scale * inp_open * xin
    coeff = jnp.concatenate([decay_mult[1:], jnp.ones((1, col_count), jnp.float32)], axis=0)
    prod_after, local_part = lax.associative_scan(compose, (coeff, upstream), reverse=True, axis=0)
    alpha_part = decay_mult[0] * local_part[0]
    beta_part = decay_mult[0] * prod_after[0]
    carried = prefix(
        (beta_part, alpha_part),
        "sp",
        chain_join,
        (jnp.ones_like(beta_part), jnp.zeros_like(alpha_part)),
    )
    incoming = carried[1]
    dstate = local_part + prod_after * incoming[None, :]
    scale_slope = jnp.where(spare_room > 0.01, -decay_mult * decay_mult / in_scale, 0.0)
    log_grad = dstate * (
        memory_hidden_values.astype(jnp.float32) - drive + scale_slope * inp_open * xin
    )
    grad_rec = (
        log_grad
        * (-8.0 * feature_fading_speed[None, :])
        * memory_switch_fraction
        * (1.0 - memory_switch_fraction)
    ).astype(jnp.bfloat16)
    grad_in = (dstate * in_scale * xin * inp_open * (1.0 - inp_open)).astype(jnp.bfloat16)
    back_rec = jnp.einsum(
        "tnd,ncd->tnc",
        grad_rec.reshape(tok_rows, blocks_here, block_width),
        memory_switch_tiles,
        preferred_element_type=jnp.float32,
    )
    back_in = jnp.einsum(
        "tnd,ncd->tnc",
        grad_in.reshape(tok_rows, blocks_here, block_width),
        entry_switch_tiles,
        preferred_element_type=jnp.float32,
    )
    lru_input_grad = (
        dstate * in_scale * inp_open
        + back_rec.reshape(tok_rows, col_count)
        + back_in.reshape(tok_rows, col_count)
    )
    columns = mixed_grad
    out_proj_grad = lax.psum_scatter(
        jnp.einsum("tr,tc->rc", columns, memory_hidden_values, preferred_element_type=jnp.float32),
        "sp",
        scatter_dimension=0,
        tiled=True,
    )
    return (
        gate_weight_grad[None],
        up_weight_grad[None],
        down_grad[None],
        out_proj_grad,
        lru_input_grad,
    )


def solution(mesh):
    return jax.shard_map(
        local,
        mesh=mesh,
        in_specs=(
            P("sp", None),
            P("sp", None),
            P("sp", None),
            P("sp", None),
            P("sp", None, "tp"),
            P("sp", None, "tp"),
            P("sp", "tp", None),
            P("sp", "tp"),
            P("sp", "tp"),
            P("sp", "tp"),
            P("tp"),
            P("sp"),
            P("tp", None, None),
            P("tp", None, None),
        ),
        out_specs=(
            P("sp", None, "tp"),
            P("sp", None, "tp"),
            P("sp", "tp", None),
            P("sp", "tp"),
            P("sp", "tp"),
        ),
        check_vma=False,
    )
```

profile of v0, /device:TPU:0, one launch (start us, length us, event | category | flops | bytes accessed | tf_op | source)
XLA Modules:
  0.0 415.6 jit_solution(13920813753677419819)
XLA Ops:
  8.1 0.8 add_multiply_fusion.12
  8.9 0.8 copy.49
  9.7 0.1 eq.29
  9.8 0.1 eq.25
  9.9 0.1 copy.53
  10.1 0.1 mul.272
  10.2 1.2 reduce-window.6
  11.8 0.1 copy.48
  11.9 0.1 mul.267
  12.1 1.7 broadcast_in_dim.22
  13.8 1.2 reshape.168
  15.0 3.0 scatter_custom_fusion
  18.0 4.2 %scatter_custom_fusion.1 = bf16[1024,512]{1,0:T(8,128)(2,1)} fusion(bf16[1024,512]{1,0:T(8,128)(2,1)} %scatter_custom_fusion, s32[256]{0:T(256)S(1)} %bitcast.121, bf16[256,2048]{1,0:T(8,128)(2,1)} %reshape.168, s32[]{:T(128)} %constant.77.clone.1, s32[]{:T(128)S(6)} %select_n.47), kind=kCustom, calls=%fused_computation.72 | custom fusion | bytes 1311236 | tf_op jit(solution)/shard_map/scatter | solution.py:72
  22.3 33.3 %all_to_all.15 = bf16[8,128,512]{2,1,0:T(8,128)(2,1)} all-to-all(bf16[8,128,512]{2,1,0:T(8,128)(2,1)} %bitcast.7), channel_id=1, replica_groups=mesh['sp'=8,'tp'=4] {'sp'}, dimensions={0} | all-to-all | bytes 2097152 | tf_op jit(solution)/shard_map/all_to_all | solution.py:131
  55.6 2.4 mul.275
  58.1 3.8 mul.276
  62.0 0.1 mul.273
  62.1 3.3 scatter_custom_fusion.2
  65.4 4.4 %scatter_custom_fusion.3 = bf16[1024,512]{1,0:T(8,128)(2,1)} fusion(bf16[1024,512]{1,0:T(8,128)(2,1)} %scatter_custom_fusion.2, s32[256]{0:T(256)S(1)} %bitcast.122, f32[256,2048]{1,0:T(8,128)} %mul.276, s32[]{:T(128)S(6)} %select_n.47, f32[256]{0:T(256)S(1)} %mul.273), kind=kCustom, calls=%fused_computation.154 | custom fusion | flops 262144 | bytes 1573892 | tf_op jit(solution)/shard_map/scatter | solution.py:72
  69.8 29.7 %all_to_all.16 = bf16[8,128,512]{2,1,0:T(8,128)(2,1)} all-to-all(bf16[8,128,512]{2,1,0:T(8,128)(2,1)} %bitcast.106), channel_id=1, replica_groups=mesh['sp'=8,'tp'=4] {'sp'}, dimensions={0} | all-to-all | bytes 2097152 | tf_op jit(solution)/shard_map/all_to_all | solution.py:124
  99.5 5.7 %fusion.5 = f32[1024,448]{0,1:T(8,128)} fusion(bf16[1024,2048]{1,0:T(8,128)(2,1)} %bitcast.125, bf16[1,2048,448]{1,2,0:T(8,128)(2,1)S(1)} %copy-done), kind=kOutput, calls=%fused_computation.19 | convolution fusion | flops 1879048192 | bytes 7864320 | tf_op jit(solution)/shard_map/dot_general | solution.py:39
  105.2 3.4 fusion.8
  108.5 24.5 %all-gather.8.cloned.1.call-done = bf16[8,128,2048]{2,1,0:T(8,128)(2,1)} async-done(((bf16[8,128,512]{2,1,0:T(8,128)(2,1)}), bf16[8,128,2048]{2,1,0:T(8,128)(2,1)}) %all-gather.8.cloned.1.call-update) | async-done | bytes 4194320 | tf_op jit(solution)/shard_map/all_gather | solution.py:140
  133.1 6.4 %multiply_convert_fusion.1 = (bf16[1024,448]{0,1:T(8,128)(2,1)S(1)}, bf16[1024,448]{0,1:T(8,128)(2,1)S(1)}) fusion(f32[1024,448]{0,1:T(8,128)} %fusion.5, f32[1024,448]{0,1:T(8,128)} %fusion.8, bf16[1024,2048]{1,0:T(8,128)(2,1)} %bitcast.129, bf16[1,448,2048]{2,1,0:T(8,128)(2,1)} %param.24), kind=kOutput, calls=%fused_computation.27 | convolution fusion | flops 1885011968 | bytes 11534336 | tf_op jit(solution)/shard_map/rd,fd->rf/dot_general | solution.py:46
  139.5 2.4 fusion.3
  142.0 4.5 %add_convert_fusion = bf16[1024,2048]{1,0:T(8,128)(2,1)} fusion(f32[1024,2048]{1,0:T(8,128)S(1)} %fusion.3, bf16[1024,448]{0,1:T(8,128)(2,1)S(1)} %get-tuple-element.109, bf16[1,2048,448]{1,2,0:T(8,128)(2,1)S(1)} %copy-done.15), kind=kOutput, calls=%fused_computation.9 | convolution fusion | flops 1883242496 | bytes 15335424 | tf_op jit(solution)/shard_map/rf,df->rd/dot_general | solution.py:56
  146.5 5.5 %all-to-all-start.2 = ((bf16[8,128,2048]{2,1,0:T(8,128)(2,1)}), bf16[8,128,2048]{2,1,0:T(8,128)(2,1)}, u32[]{:S(2)}, u32[]{:S(2)}) async-start(bf16[8,128,2048]{2,1,0:T(8,128)(2,1)} %bitcast.105), calls=%async_computation.2 | async-start | bytes 8388608 | tf_op jit(solution)/shard_map/all_to_all | solution.py:152
  152.0 0.2 all-reduce.32.cloned.1.call-start
  152.2 93.4 %all-to-all-done.2 = bf16[8,128,2048]{2,1,0:T(8,128)(2,1)} async-done(((bf16[8,128,2048]{2,1,0:T(8,128)(2,1)}), bf16[8,128,2048]{2,1,0:T(8,128)(2,1)}, u32[]{:S(2)}, u32[]{:S(2)}) %all-to-all-start.2) | async-done | bytes 4194336 | tf_op jit(solution)/shard_map/all_to_all | solution.py:152
  245.7 6.1 %gather_fusion.1 = bf16[256,2048]{1,0:T(8,128)(2,1)} fusion(bf16[1024,2048]{1,0:T(8,128)(2,1)} %bitcast.18, s32[1024]{0:T(1024)S(1)} %get-tuple-element.150), kind=kCustom, calls=%fused_computation.1.clone | custom fusion | bytes 2098176 | tf_op jit(solution)/shard_map/jit(_take)/gather | solution.py:65
  251.7 6.1 %gather_fusion = bf16[256,2048]{1,0:T(8,128)(2,1)} fusion(bf16[1024,2048]{1,0:T(8,128)(2,1)} %bitcast.18, s32[1024]{0:T(1024)S(1)} %get-tuple-element.151), kind=kCustom, calls=%fused_computation.clone | custom fusion | bytes 2098176 | tf_op jit(solution)/shard_map/jit(_take)/gather | solution.py:63
  257.8 1.9 convert_add_fusion
  259.7 2.3 reshape.175
  262.0 5.0 %reduce_sum.22 = bf16[128,2048]{1,0:T(8,128)(2,1)} reduce(f32[128,2,2048]{2,1,0:T(2,128)} %reshape.175, f32[]{:T(128)} %constant.87.clone.1), dimensions={1}, to_apply=%region_7.9 | reduce | flops 262144 | bytes 2621444 | tf_op jit(solution)/shard_map/reduce_sum | solution.py:66
  267.1 0.5 all-gather.10.cloned.1.call-update
  267.7 0.3 reduce-scatter.2.cloned.1.call-start
  268.0 0.3 fusion.18
  268.3 0.1 copy.67
  268.9 0.3 fusion.15
  269.2 0.1 copy.68
  269.4 0.2 slice.246
  269.5 0.1 slice.250
  269.7 0.1 slice.256
  269.8 5.9 %fusion.1 = bf16[1,2048,448]{1,2,0:T(8,128)(2,1)} fusion(bf16[1024,448]{0,1:T(8,128)(2,1)} %copy-done.16, bf16[1024,2048]{1,0:T(8,128)(2,1)} %bitcast.126), kind=kOutput, calls=%fused_computation.14 | convolution fusion | flops 1879965696 | bytes 6946816 | tf_op jit(solution)/shard_map/rd,rf->df/dot_general | solution.py:49
  275.7 23.1 %all-reduce.32.cloned.1.call-done = bf16[128,2048]{1,0:T(8,128)(2,1)} async-done(((bf16[128,2048]{1,0:T(8,128)(2,1)}), bf16[128,2048]{1,0:T(8,128)(2,1)}) %all-reduce.32.cloned.1.call-update) | async-done | bytes 524304 | tf_op jit(solution)/shard_map/psum | solution.py:160
  298.8 3.8 fusion.44
  302.6 1.2 copy-done.18
  303.8 5.6 %fusion.2 = bf16[1,2048,448]{1,2,0:T(8,128)(2,1)} fusion(bf16[1024,448]{0,1:T(8,128)(2,1)S(1)} %copy-done.18, bf16[1024,2048]{1,0:T(8,128)(2,1)} %bitcast.127), kind=kOutput, calls=%fused_computation.15 | convolution fusion | flops 1879965696 | bytes 6946816 | tf_op jit(solution)/shard_map/rd,rf->df/dot_general | solution.py:52
  309.4 3.4 fusion
  312.8 4.0 all-gather.10.cloned.1.call-done
  316.8 2.0 fusion.43
  319.0 0.1 slice.248
  319.2 0.1 slice.252
  321.1 0.2 slice.243
  321.6 0.1 rev.8
  321.9 0.1 rev.9
  322.1 27.2 %all-gather = f32[8,1,512]{2,1,0:T(1,128)S(1)} all-gather(f32[1,1,512]{2,1,0:T(1,128)S(1)} %get-tuple-element.113), channel_id=1, replica_groups=mesh['sp'=8,'tp'=4] {'sp'}, dimensions={0}, use_global_device_ids=true | all-gather | bytes 18432 | tf_op jit(solution)/shard_map/all_gather | solution.py:13
  349.3 26.6 %all-gather.1 = f32[8,1,512]{2,1,0:T(1,128)S(1)} all-gather(f32[1,1,512]{2,1,0:T(1,128)S(1)} %get-tuple-element.112), channel_id=1, replica_groups=mesh['sp'=8,'tp'=4] {'sp'}, dimensions={0}, use_global_device_ids=true | all-gather | bytes 18432 | tf_op jit(solution)/shard_map/all_gather | solution.py:13
  375.9 0.3 while.14
  376.3 0.5 fusion.34
  376.8 0.2 convolution_bitcast_fusion
  377.1 0.2 convolution_bitcast_fusion.1
  377.3 0.8 add_add_fusion
  378.1 30.1 %reduce-scatter.2.cloned.1.call-done = f32[256,512]{1,0:T(8,128)} async-done(((f32[2048,512]{1,0:T(8,128)}), f32[256,512]{1,0:T(8,128)}) %reduce-scatter.2.cloned.1.call-update) | async-done | bytes 524304 | tf_op jit(solution)/shard_map/reduce_scatter | solution.py:231
  (191 shorter events, 3.5 us)
Async XLA Ops:
  8.0 91.5 %copy-start = (bf16[1,2048,448]{1,2,0:T(8,128)(2,1)S(1)}, bf16[1,2048,448]{1,2,0:T(8,128)(2,1)}, u32[]{:S(2)}) copy-start(bf16[1,2048,448]{1,2,0:T(8,128)(2,1)} %param.22) | copy-start | bytes 5505028
  8.0 91.5 %all-gather.6.cloned.1.call-start = ((), (), s32[]{:S(2)}) async-start(), calls=%async_computation.4 | async-start | bytes 5242880 | tf_op jit(solution)/shard_map/all_gather | solution.py:141
  22.3 33.4 %copy-start.2 = (bf16[128,2048]{1,0:T(8,128)(2,1)S(1)}, bf16[128,2048]{1,0:T(8,128)(2,1)}, u32[]{:S(2)}) copy-start(bf16[128,2048]{1,0:T(8,128)(2,1)} %param.18) | copy-start | bytes 1572868
  55.6 77.5 %all-gather.8.cloned.1.call-start = ((), (), s32[]{:S(2)}) async-start(), calls=%async_computation.5 | async-start | bytes 5242880 | tf_op jit(solution)/shard_map/all_gather | solution.py:140
  58.1 3.8 copy-start.11
  99.5 5.7 %copy-start.12 = (bf16[8,128,2048]{2,1,0:T(8,128)(2,1)S(1)}, bf16[8,128,2048]{2,1,0:T(8,128)(2,1)}, u32[]{:S(2)}) copy-start(bf16[8,128,2048]{2,1,0:T(8,128)(2,1)} %all-gather.6.cloned.1.call-done) | copy-start | bytes 12582916
  99.5 5.7 %copy-start.14 = (bf16[1,2048,448]{1,2,0:T(8,128)(2,1)S(1)}, bf16[1,2048,448]{1,2,0:T(8,128)(2,1)}, u32[]{:S(2)}) copy-start(bf16[1,2048,448]{1,2,0:T(8,128)(2,1)} %param.23) | copy-start | bytes 5505028
  139.5 2.5 copy-start.16
  139.5 2.5 copy-start.17
  139.5 2.5 copy-start.15
  146.5 99.2 %all-to-all-start.2 = ((bf16[8,128,2048]{2,1,0:T(8,128)(2,1)}), bf16[8,128,2048]{2,1,0:T(8,128)(2,1)}, u32[]{:S(2)}, u32[]{:S(2)}) async-start(bf16[8,128,2048]{2,1,0:T(8,128)(2,1)} %bitcast.105), calls=%async_computation.2 | async-start | bytes 8388608 | tf_op jit(solution)/shard_map/all_to_all | solution.py:152
  152.0 146.8 %all-reduce.32.cloned.1.call-start = ((), (), s32[]{:S(2)}) async-start(), calls=%async_computation.6 | async-start | bytes 1048576 | tf_op jit(solution)/shard_map/psum | solution.py:160
  262.0 5.9 %copy-start.6 = (bf16[2,256,256]{2,1,0:T(8,128)(2,1)S(1)}, bf16[2,256,256]{2,1,0:T(8,128)(2,1)}, u32[]{:S(2)}) copy-start(bf16[2,256,256]{2,1,0:T(8,128)(2,1)} %param.30) | copy-start | bytes 786436
  262.0 5.9 %copy-start.7 = (bf16[128,512]{1,0:T(8,128)(2,1)S(1)}, bf16[128,512]{1,0:T(8,128)(2,1)}, u32[]{:S(2)}) copy-start(bf16[128,512]{1,0:T(8,128)(2,1)} %param.26) | copy-start | bytes 393220
  267.1 1.3 copy-start.9
  267.1 1.4 copy-start.10
  267.1 49.7 %all-gather.10.cloned.1.call-start = ((), (), s32[]{:S(2)}) async-start(), calls=%async_computation.8 | async-start | bytes 2359296 | tf_op jit(solution)/shard_map/all_gather | solution.py:166
  267.7 140.6 %reduce-scatter.2.cloned.1.call-start = ((), (), s32[]{:S(2)}) async-start(), calls=%async_computation.7 | async-start | bytes 4718592 | tf_op jit(solution)/shard_map/reduce_scatter | solution.py:231
  267.9 1.0 copy-start.5
  269.8 29.0 %copy-start.4 = (bf16[128,512]{1,0:T(8,128)(2,1)S(1)}, bf16[128,512]{1,0:T(8,128)(2,1)}, u32[]{:S(2)}) copy-start(bf16[128,512]{1,0:T(8,128)(2,1)} %param.27) | copy-start | bytes 393220
  302.6 1.2 copy-start.18
  303.7 5.6 %copy-start.13 = (bf16[8,128,2048]{2,1,0:T(8,128)(2,1)S(1)}, bf16[8,128,2048]{2,1,0:T(8,128)(2,1)}, u32[]{:S(2)}) copy-start(bf16[8,128,2048]{2,1,0:T(8,128)(2,1)} %all-gather.8.cloned.1.call-done) | copy-start | bytes 12582916
  303.7 5.6 %copy-start.19 = (f32[1024,448]{0,1:T(8,128)S(1)}, f32[1024,448]{0,1:T(8,128)}, u32[]{:S(2)}) copy-start(f32[1024,448]{0,1:T(8,128)} %fusion.5) | copy-start | bytes 5505028
  303.8 5.6 %copy-start.20 = (f32[1024,448]{0,1:T(8,128)S(1)}, f32[1024,448]{0,1:T(8,128)}, u32[]{:S(2)}) copy-start(f32[1024,448]{0,1:T(8,128)} %fusion.8) | copy-start | bytes 5505028
  309.4 7.4 %copy-start.3 = (bf16[128,2048]{1,0:T(8,128)(2,1)S(1)}, bf16[128,2048]{1,0:T(8,128)(2,1)}, u32[]{:S(2)}) copy-start(bf16[128,2048]{1,0:T(8,128)(2,1)} %all-reduce.32.cloned.1.call-done) | copy-start | bytes 1572868
  321.6 54.7 %copy-start.8 = (bf16[128,512]{1,0:T(8,128)(2,1)S(1)}, bf16[128,512]{1,0:T(8,128)(2,1)}, u32[]{:S(2)}) copy-start(bf16[128,512]{1,0:T(8,128)(2,1)} %param.26) | copy-start | bytes 393220
  376.8 31.4 %copy-start.1 = (bf16[1,2048,448]{1,2,0:T(8,128)(2,1)S(1)}, bf16[1,2048,448]{1,2,0:T(8,128)(2,1)}, u32[]{:S(2)}) copy-start(bf16[1,2048,448]{1,2,0:T(8,128)(2,1)} %param.22) | copy-start | bytes 5505028
Sparse Core Ops, SparseCore 0:
  55.7 33.4 all-gather.5
  99.6 33.4 all-gather.7
  267.2 31.5 all-reduce.31
Sparse Core Ops, SparseCore 1:
  269.7 47.0 all-gather.9
  320.8 87.3 reduce-scatter.1
where the time goes:
time: 423 us; the launch traced here: 416 us
  waiting for transfers between devices  176 us (42%)
  blocking collectives  117 us (28%)
  matrix products  44.1 us (10%)
  local copies, waits for them, and re-layouts  37.3 us (9%)
  other arithmetic  18.9 us (4%)
  between operations  16.5 us (4%)
  starting transfers between devices  6.08 us (1%)
    all_to_all x1, waiting for transfers between devices, local(): lax.all_to_all(token_part.astype(jnp.bfloat16).reshape(sp_count, capacity...  93.4 us
    all_gather x2, blocking collectives, prefix(): gathered = jax.tree.map(lambda a: lax.all_gather(a, axis), part)  53.8 us
    all_to_all x1, blocking collectives, local(): lax.all_to_all(send_rows.reshape(sp_count, capacity, share), 'sp', split_...  33.3 us
    reduce_scatter x1, waiting for transfers between devices, local(): lax.psum_scatter(jnp.einsum('tr,tc->rc', columns, memory_hidden_values, p...  30.1 us
    all_to_all x1, blocking collectives, local(): lax.all_to_all(send_grad.reshape(sp_count, capacity, share), 'sp', split_...  29.7 us
    all_gather x1, waiting for transfers between devices, local(): lax.all_gather(got_grad, 'tp', axis=2, tiled=True)  24.5 us
    psum x1, waiting for transfers between devices, local(): moe_grad = lax.psum(own_sum.astype(jnp.bfloat16), 'tp').astype(jnp.float32)  23.1 us
  transfers between devices with their start and end apart: 6, of which 5 were waited for; matrix products, arithmetic and copies ran while one was open for 12% of the time, Pallas kernels for 0%

commit v1 on v0

--- a/solution.py
+++ b/solution.py
@@ -157,7 +157,9 @@
         tiled=True,
     )
     own_sum = collect(returned.reshape(slot_rows, feature_count), targets, route_count)
-    moe_grad = lax.psum(own_sum.astype(jnp.bfloat16), "tp").astype(jnp.float32)
+    moe_grad = jnp.sum(lax.all_gather(own_sum.astype(jnp.bfloat16), "tp"), axis=0).astype(
+        jnp.float32
+    )
     mixed_grad = (result_cotangent_values.astype(jnp.float32) + moe_grad).astype(jnp.bfloat16)
     col_count = memory_readout_map.shape[1]
     columns = mixed_grad

time: 423 us -> 444 us (1.050)
  waiting for transfers between devices: 176 us -> 198 us
    all_gather x1, waiting for transfers between devices: 4 us -> 37 us  [local(): lax.all_gather(memory_readout_map, 'sp', axis=0, tiled=True)]
    psum x1 -> x0, waiting for transfers between devices: 23.1 us -> none  [local(): moe_grad = lax.psum(own_sum.astype(jnp.bfloat16), 'tp').astype(jnp.float32)]
    all_gather x0 -> x1, waiting for transfers between devices: none -> 12.1 us  [local(): lax.all_gather(own_sum.astype(jnp.bfloat16), 'tp')]
where the time goes in v1:
time: 444 us; the launch traced here: 436 us
  waiting for transfers between devices  198 us (45%)
  blocking collectives  117 us (26%)
  matrix products  43.4 us (10%)
  local copies, waits for them, and re-layouts  36.1 us (8%)
  other arithmetic  21 us (5%)
  between operations  15.1 us (3%)
  starting transfers between devices  6.1 us (1%)
    all_to_all x1, waiting for transfers between devices, local(): lax.all_to_all(token_part.astype(jnp.bfloat16).reshape(sp_count, capacity...  93.4 us
    all_gather x2, blocking collectives, prefix(): gathered = jax.tree.map(lambda a: lax.all_gather(a, axis), part)  53.8 us
    all_gather x1, waiting for transfers between devices, local(): lax.all_gather(memory_readout_map, 'sp', axis=0, tiled=True)  37 us
    all_to_all x1, blocking collectives, local(): lax.all_to_all(send_rows.reshape(sp_count, capacity, share), 'sp', split_...  33.3 us
    reduce_scatter x1, waiting for transfers between devices, local(): lax.psum_scatter(jnp.einsum('tr,tc->rc', columns, memory_hidden_values, p...  30.1 us
    all_to_all x1, blocking collectives, local(): lax.all_to_all(send_grad.reshape(sp_count, capacity, share), 'sp', split_...  29.7 us
    all_gather x1, waiting for transfers between devices, local(): lax.all_gather(got_grad, 'tp', axis=2, tiled=True)  24.5 us
    all_gather x1, waiting for transfers between devices, local(): lax.all_gather(own_sum.astype(jnp.bfloat16), 'tp')  12.1 us
  transfers between devices with their start and end apart: 6, of which 5 were waited for; matrix products, arithmetic and copies ran while one was open for 12% of the time, Pallas kernels for 0%

profile of v1, /device:TPU:0, one launch (start us, length us, event | category | flops | bytes accessed | tf_op | source)
XLA Modules:
  0.0 436.3 jit_solution(13711979868662004435)
XLA Ops:
  7.2 0.8 add_multiply_fusion.12
  8.0 0.8 copy.66
  8.8 0.1 eq.29
  9.0 0.1 eq.25
  9.1 0.1 copy.70
  9.2 0.1 mul.272
  9.4 1.2 reduce-window.6
  11.1 0.1 mul.267
  11.3 1.7 broadcast_in_dim.22
  12.9 1.2 reshape.176
  14.2 3.0 scatter_custom_fusion
  17.2 4.2 scatter_custom_fusion.1
  21.4 33.3 %all_to_all.15 = bf16[8,128,512]{2,1,0:T(8,128)(2,1)} all-to-all(bf16[8,128,512]{2,1,0:T(8,128)(2,1)} %bitcast.7), channel_id=1, replica_groups=mesh['sp'=8,'tp'=4] {'sp'}, dimensions={0} | all-to-all | bytes 2097152 | tf_op jit(solution)/shard_map/all_to_all | solution.py:131
  54.8 2.4 mul.275
  57.2 3.8 mul.276
  61.0 0.1 copy.71
  61.1 0.1 mul.273
  61.3 3.3 scatter_custom_fusion.2
  64.5 4.4 %scatter_custom_fusion.3 = bf16[1024,512]{1,0:T(8,128)(2,1)} fusion(bf16[1024,512]{1,0:T(8,128)(2,1)} %scatter_custom_fusion.2, s32[256]{0:T(256)S(1)} %bitcast.124, f32[256,2048]{1,0:T(8,128)} %mul.276, s32[]{:T(128)S(6)} %select_n.47, f32[256]{0:T(256)S(1)} %mul.273), kind=kCustom, calls=%fused_computation.154 | custom fusion | flops 262144 | bytes 1573892 | tf_op jit(solution)/shard_map/scatter | solution.py:72
  68.9 29.7 %all_to_all.16 = bf16[8,128,512]{2,1,0:T(8,128)(2,1)} all-to-all(bf16[8,128,512]{2,1,0:T(8,128)(2,1)} %bitcast.107), channel_id=1, replica_groups=mesh['sp'=8,'tp'=4] {'sp'}, dimensions={0} | all-to-all | bytes 2097152 | tf_op jit(solution)/shard_map/all_to_all | solution.py:124
  98.7 5.7 %fusion.5 = f32[1024,448]{0,1:T(8,128)} fusion(bf16[1024,2048]{1,0:T(8,128)(2,1)} %bitcast.127, bf16[1,2048,448]{1,2,0:T(8,128)(2,1)S(1)} %copy-done), kind=kOutput, calls=%fused_computation.19 | convolution fusion | flops 1879048192 | bytes 7864320 | tf_op jit(solution)/shard_map/dot_general | solution.py:39
  104.3 3.4 fusion.8
  107.7 24.5 %all-gather.10.cloned.1.call-done = bf16[8,128,2048]{2,1,0:T(8,128)(2,1)} async-done(((bf16[8,128,512]{2,1,0:T(8,128)(2,1)}), bf16[8,128,2048]{2,1,0:T(8,128)(2,1)}) %all-gather.10.cloned.1.call-update) | async-done | bytes 4194320 | tf_op jit(solution)/shard_map/all_gather | solution.py:140
  132.2 6.4 %multiply_convert_fusion.1 = (bf16[1024,448]{0,1:T(8,128)(2,1)S(1)}, bf16[1024,448]{0,1:T(8,128)(2,1)S(1)}) fusion(f32[1024,448]{0,1:T(8,128)} %fusion.5, f32[1024,448]{0,1:T(8,128)} %fusion.8, bf16[1024,2048]{1,0:T(8,128)(2,1)} %bitcast.131, bf16[1,448,2048]{2,1,0:T(8,128)(2,1)} %param.24), kind=kOutput, calls=%fused_computation.27 | convolution fusion | flops 1885011968 | bytes 11534336 | tf_op jit(solution)/shard_map/rd,fd->rf/dot_general | solution.py:46
  138.7 2.4 fusion.3
  141.1 4.5 %add_convert_fusion = bf16[1024,2048]{1,0:T(8,128)(2,1)} fusion(f32[1024,2048]{1,0:T(8,128)S(1)} %fusion.3, bf16[1024,448]{0,1:T(8,128)(2,1)S(1)} %get-tuple-element.109, bf16[1,2048,448]{1,2,0:T(8,128)(2,1)S(1)} %copy-done.13), kind=kOutput, calls=%fused_computation.9 | convolution fusion | flops 1883242496 | bytes 15335424 | tf_op jit(solution)/shard_map/rf,df->rd/dot_general | solution.py:56
  145.6 5.5 %all-to-all-start.2 = ((bf16[8,128,2048]{2,1,0:T(8,128)(2,1)}), bf16[8,128,2048]{2,1,0:T(8,128)(2,1)}, u32[]{:S(2)}, u32[]{:S(2)}) async-start(bf16[8,128,2048]{2,1,0:T(8,128)(2,1)} %bitcast.106), calls=%async_computation.2 | async-start | bytes 8388608 | tf_op jit(solution)/shard_map/all_to_all | solution.py:152
  151.2 0.2 all-gather.14.cloned.1.call-start
  151.4 93.4 %all-to-all-done.2 = bf16[8,128,2048]{2,1,0:T(8,128)(2,1)} async-done(((bf16[8,128,2048]{2,1,0:T(8,128)(2,1)}), bf16[8,128,2048]{2,1,0:T(8,128)(2,1)}, u32[]{:S(2)}, u32[]{:S(2)}) %all-to-all-start.2) | async-done | bytes 4194336 | tf_op jit(solution)/shard_map/all_to_all | solution.py:152
  244.9 6.1 %gather_fusion.1 = bf16[256,2048]{1,0:T(8,128)(2,1)} fusion(bf16[1024,2048]{1,0:T(8,128)(2,1)} %bitcast.18, s32[1024]{0:T(1024)S(1)} %get-tuple-element.150), kind=kCustom, calls=%fused_computation.1.clone | custom fusion | bytes 2098176 | tf_op jit(solution)/shard_map/jit(_take)/gather | solution.py:65
  250.9 6.1 %gather_fusion = bf16[256,2048]{1,0:T(8,128)(2,1)} fusion(bf16[1024,2048]{1,0:T(8,128)(2,1)} %bitcast.18, s32[1024]{0:T(1024)S(1)} %get-tuple-element.151), kind=kCustom, calls=%fused_computation.clone | custom fusion | bytes 2098176 | tf_op jit(solution)/shard_map/jit(_take)/gather | solution.py:63
  257.0 1.9 convert_add_fusion
  258.9 2.3 reshape.183
  261.2 5.0 %reduce_sum.34 = bf16[128,2048]{1,0:T(8,128)(2,1)} reduce(f32[128,2,2048]{2,1,0:T(2,128)} %reshape.183, f32[]{:T(128)} %constant.88.clone.1), dimensions={1}, to_apply=%region_7.9 | reduce | flops 262144 | bytes 2621444 | tf_op jit(solution)/shard_map/reduce_sum | solution.py:66
  266.3 0.5 all-gather.12.cloned.1.call-update
  266.8 0.3 reduce-scatter.2.cloned.1.call-start
  267.1 0.3 fusion.18
  267.4 0.1 copy.84
  268.1 0.3 fusion.15
  268.4 0.1 copy.85
  268.6 0.2 slice.246
  268.7 0.1 slice.250
  268.8 0.1 slice.256
  269.0 6.0 %fusion.1 = bf16[1,2048,448]{1,2,0:T(8,128)(2,1)} fusion(bf16[1024,448]{0,1:T(8,128)(2,1)} %copy-done.14, bf16[1024,2048]{1,0:T(8,128)(2,1)} %bitcast.128), kind=kOutput, calls=%fused_computation.14 | convolution fusion | flops 1879965696 | bytes 6946816 | tf_op jit(solution)/shard_map/rd,rf->df/dot_general | solution.py:49
  275.0 12.1 %all-gather.14.cloned.1.call-done = bf16[512,2048]{1,0:T(8,128)(2,1)} async-done(((bf16[128,2048]{1,0:T(8,128)(2,1)}), bf16[512,2048]{1,0:T(8,128)(2,1)}) %all-gather.14.cloned.1.call-update) | async-done | bytes 2097168 | tf_op jit(solution)/shard_map/all_gather | solution.py:160
  287.1 2.0 reduce_sum.35
  289.1 2.7 fusion.44
  291.9 5.9 %fusion.2 = bf16[1,2048,448]{1,2,0:T(8,128)(2,1)} fusion(bf16[1024,448]{0,1:T(8,128)(2,1)} %copy-done.15, bf16[1024,2048]{1,0:T(8,128)(2,1)} %bitcast.129), kind=kOutput, calls=%fused_computation.15 | convolution fusion | flops 1879965696 | bytes 6946816 | tf_op jit(solution)/shard_map/rd,rf->df/dot_general | solution.py:52
  297.9 3.4 fusion
  301.2 37.0 %all-gather.12.cloned.1.call-done = bf16[2048,512]{1,0:T(8,128)(2,1)} async-done(((bf16[256,512]{1,0:T(8,128)(2,1)}), bf16[2048,512]{1,0:T(8,128)(2,1)}) %all-gather.12.cloned.1.call-update) | async-done | bytes 2097168 | tf_op jit(solution)/shard_map/all_gather | solution.py:168
  338.2 2.0 fusion.43
  340.5 0.1 slice.248
  340.6 0.1 slice.252
  342.5 0.2 slice.243
  343.0 0.1 rev.8
  343.3 0.1 rev.9
  343.5 27.1 %all-gather.1 = f32[8,1,512]{2,1,0:T(1,128)S(1)} all-gather(f32[1,1,512]{2,1,0:T(1,128)S(1)} %get-tuple-element.113), channel_id=1, replica_groups=mesh['sp'=8,'tp'=4] {'sp'}, dimensions={0}, use_global_device_ids=true | all-gather | bytes 18432 | tf_op jit(solution)/shard_map/all_gather | solution.py:13
  370.7 26.6 %all-gather.2 = f32[8,1,512]{2,1,0:T(1,128)S(1)} all-gather(f32[1,1,512]{2,1,0:T(1,128)S(1)} %get-tuple-element.112), channel_id=1, replica_groups=mesh['sp'=8,'tp'=4] {'sp'}, dimensions={0}, use_global_device_ids=true | all-gather | bytes 18432 | tf_op jit(solution)/shard_map/all_gather | solution.py:13
  397.3 0.3 while.14
  397.6 0.5 fusion.34
  398.2 0.2 convolution_bitcast_fusion
  398.4 0.2 convolution_bitcast_fusion.1
  398.7 0.8 add_add_fusion
  399.5 30.1 %reduce-scatter.2.cloned.1.call-done = f32[256,512]{1,0:T(8,128)} async-done(((f32[2048,512]{1,0:T(8,128)}), f32[256,512]{1,0:T(8,128)}) %reduce-scatter.2.cloned.1.call-update) | async-done | bytes 524304 | tf_op jit(solution)/shard_map/reduce_scatter | solution.py:233
  (186 shorter events, 3.5 us)
Async XLA Ops:
  7.2 91.5 %copy-start = (bf16[1,2048,448]{1,2,0:T(8,128)(2,1)S(1)}, bf16[1,2048,448]{1,2,0:T(8,128)(2,1)}, u32[]{:S(2)}) copy-start(bf16[1,2048,448]{1,2,0:T(8,128)(2,1)} %param.22) | copy-start | bytes 5505028
  7.2 91.5 %all-gather.8.cloned.1.call-start = ((), (), s32[]{:S(2)}) async-start(), calls=%async_computation.4 | async-start | bytes 5242880 | tf_op jit(solution)/shard_map/all_gather | solution.py:141
  21.4 33.4 %copy-start.2 = (bf16[128,2048]{1,0:T(8,128)(2,1)S(1)}, bf16[128,2048]{1,0:T(8,128)(2,1)}, u32[]{:S(2)}) copy-start(bf16[128,2048]{1,0:T(8,128)(2,1)} %param.18) | copy-start | bytes 1572868
  54.7 77.5 %all-gather.10.cloned.1.call-start = ((), (), s32[]{:S(2)}) async-start(), calls=%async_computation.5 | async-start | bytes 5242880 | tf_op jit(solution)/shard_map/all_gather | solution.py:140
  57.2 3.8 copy-start.9
  98.7 5.7 %copy-start.10 = (bf16[8,128,2048]{2,1,0:T(8,128)(2,1)S(1)}, bf16[8,128,2048]{2,1,0:T(8,128)(2,1)}, u32[]{:S(2)}) copy-start(bf16[8,128,2048]{2,1,0:T(8,128)(2,1)} %all-gather.8.cloned.1.call-done) | copy-start | bytes 12582916
  98.7 5.7 %copy-start.12 = (bf16[1,2048,448]{1,2,0:T(8,128)(2,1)S(1)}, bf16[1,2048,448]{1,2,0:T(8,128)(2,1)}, u32[]{:S(2)}) copy-start(bf16[1,2048,448]{1,2,0:T(8,128)(2,1)} %param.23) | copy-start | bytes 5505028
  138.6 2.5 copy-start.14
  138.6 2.5 copy-start.15
  138.6 2.5 copy-start.13
  145.6 99.2 %all-to-all-start.2 = ((bf16[8,128,2048]{2,1,0:T(8,128)(2,1)}), bf16[8,128,2048]{2,1,0:T(8,128)(2,1)}, u32[]{:S(2)}, u32[]{:S(2)}) async-start(bf16[8,128,2048]{2,1,0:T(8,128)(2,1)} %bitcast.106), calls=%async_computation.2 | async-start | bytes 8388608 | tf_op jit(solution)/shard_map/all_to_all | solution.py:152
  151.2 135.9 %all-gather.14.cloned.1.call-start = ((), (), s32[]{:S(2)}) async-start(), calls=%async_computation.8 | async-start | bytes 2621440 | tf_op jit(solution)/shard_map/all_gather | solution.py:160
  261.2 5.9 %copy-start.5 = (bf16[2,256,256]{2,1,0:T(8,128)(2,1)S(1)}, bf16[2,256,256]{2,1,0:T(8,128)(2,1)}, u32[]{:S(2)}) copy-start(bf16[2,256,256]{2,1,0:T(8,128)(2,1)} %param.30) | copy-start | bytes 786436
  261.2 5.9 %copy-start.6 = (bf16[128,512]{1,0:T(8,128)(2,1)S(1)}, bf16[128,512]{1,0:T(8,128)(2,1)}, u32[]{:S(2)}) copy-start(bf16[128,512]{1,0:T(8,128)(2,1)} %param.26) | copy-start | bytes 393220
  266.2 1.3 copy-start.7
  266.2 1.4 copy-start.8
  266.3 71.9 %all-gather.12.cloned.1.call-start = ((), (), s32[]{:S(2)}) async-start(), calls=%async_computation.7 | async-start | bytes 2359296 | tf_op jit(solution)/shard_map/all_gather | solution.py:168
  266.8 162.7 %reduce-scatter.2.cloned.1.call-start = ((), (), s32[]{:S(2)}) async-start(), calls=%async_computation.6 | async-start | bytes 4718592 | tf_op jit(solution)/shard_map/reduce_scatter | solution.py:233
  267.1 1.0 copy-start.4
  275.0 14.2 %copy-start.3 = (bf16[128,512]{1,0:T(8,128)(2,1)S(1)}, bf16[128,512]{1,0:T(8,128)(2,1)}, u32[]{:S(2)}) copy-start(bf16[128,512]{1,0:T(8,128)(2,1)} %param.27) | copy-start | bytes 393220
  291.9 5.9 %copy-start.11 = (bf16[8,128,2048]{2,1,0:T(8,128)(2,1)S(1)}, bf16[8,128,2048]{2,1,0:T(8,128)(2,1)}, u32[]{:S(2)}) copy-start(bf16[8,128,2048]{2,1,0:T(8,128)(2,1)} %all-gather.10.cloned.1.call-done) | copy-start | bytes 12582916
  291.9 5.9 %copy-start.16 = (f32[1024,448]{0,1:T(8,128)S(1)}, f32[1024,448]{0,1:T(8,128)}, u32[]{:S(2)}) copy-start(f32[1024,448]{0,1:T(8,128)} %fusion.5) | copy-start | bytes 5505028
  291.9 5.9 %copy-start.17 = (f32[1024,448]{0,1:T(8,128)S(1)}, f32[1024,448]{0,1:T(8,128)}, u32[]{:S(2)}) copy-start(f32[1024,448]{0,1:T(8,128)} %fusion.8) | copy-start | bytes 5505028
  398.2 31.4 %copy-start.1 = (bf16[1,2048,448]{1,2,0:T(8,128)(2,1)S(1)}, bf16[1,2048,448]{1,2,0:T(8,128)(2,1)}, u32[]{:S(2)}) copy-start(bf16[1,2048,448]{1,2,0:T(8,128)(2,1)} %param.22) | copy-start | bytes 5505028
Sparse Core Ops, SparseCore 0:
  54.9 33.4 all-gather.7
  98.7 33.4 all-gather.9
  266.4 20.6 all-gather.13
  289.1 49.0 all-gather.11
  342.3 87.2 reduce-scatter.1
